TPU v7x, 32 devices: a whole 2x2x4 slice. The times are simulated.
32 devices in a mesh: grp: 2 (over y), dp: 2 (over x), kv: 4 (over z), tp: 2 (over core).
Axes of the slice: x: 2, y: 2, z: 4, core: 2. Of those that a mesh axis runs over, the one named last changes fastest.
Arguments:
- tokens: bfloat16 [96, 4, 4096], P(('grp', 'dp'), None, ('kv', 'tp')), parts along dimension 0, may hold values from -6 to 6
- norm_gain: float32 [4096], replicated, may hold values from 0.1 to 1.9
- w_query: bfloat16 [16, 128, 4096], P('kv', 'tp'), may hold values from -0.09375 to 0.09375
- w_key: bfloat16 [16, 128, 4096], P('kv', 'tp'), may hold values from -0.09375 to 0.09375
- w_value: bfloat16 [16, 128, 4096], P('kv', 'tp'), may hold values from -0.09375 to 0.09375
- w_gate: bfloat16 [16, 128, 4096], P('kv', 'tp'), may hold values from -0.09375 to 0.09375
- w_decay: bfloat16 [4096, 16], replicated, may hold values from -0.09375 to 0.09375
- w_beta: bfloat16 [4096, 16], replicated, may hold values from -0.09375 to 0.09375
- decay_rate: float32 [16], P('kv'), may hold values from 0.02 to 1
- head_gain: float32 [128], P('tp'), may hold values from 0.1 to 1.9
- w_out: bfloat16 [16, 128, 4096], P('kv', 'tp'), may hold values from -0.1875 to 0.1875
- state: float32 [96, 16, 128, 128], P(('grp', 'dp'), 'kv', 'tp'), parts along dimension 0, may hold values from -6 to 6
- prev_keys: bfloat16 [96, 4, 16, 128], P(('grp', 'dp'), None, 'kv'), parts along dimension 0, may hold values from -6 to 6
- prev_values: bfloat16 [96, 4, 16, 128], P(('grp', 'dp'), None, 'kv', 'tp'), parts along dimension 0, may hold values from -6 to 6
- prev_decay: float32 [96, 4, 16], P(('grp', 'dp'), None, 'kv'), parts along dimension 0, may hold values from 0.01 to 1
- prev_beta: float32 [96, 4, 16], P(('grp', 'dp'), None, 'kv'), parts along dimension 0, may hold values from 0.05 to 1
- accepted: int32 [96], P(('grp', 'dp')), parts along dimension 0, may hold values from 0 to 4
Outputs:
- mixed: bfloat16 [96, 4, 4096], P(('grp', 'dp'), None, ('kv', 'tp')), parts along dimension 0
- committed: float32 [96, 16, 128, 128], P(('grp', 'dp'), 'kv', 'tp'), parts along dimension 0
There are 2 independent parts, one for each index of `grp`. A program takes and returns all parts, laid end to end along the dimension named above; an argument that names none is the same for every part. Nothing has to cross between parts.
All inputs are finite; a program needn't handle non-finite values.
Results may differ from a plain program's by a relative error of at most 0.015.
Values may be sent and summed in bfloat16 or wider, within the bound.
A program may use at most 64 MiB of HBM per device.

v0:
```python
import functools

import jax
import jax.numpy as jnp
from jax import lax
from jax.experimental import pallas as pl
from jax.experimental.pallas import tpu as pltpu
from jax.sharding import PartitionSpec as P

EPS = 1e-06
F32 = jnp.float32
BF16 = jnp.bfloat16
MESH = pl.DeviceIdType.MESH
NT = (((1,), (1,)), ((), ()))
TN = (((0,), (0,)), ((), ()))


def dot_nt(a, b):
    return lax.dot_general(a, b, NT, preferred_element_type=F32)


def silu(u):
    return u * jax.nn.sigmoid(u)


def lane_group(rows, cols, group):
    return lax.broadcasted_iota(jnp.int32, (rows, cols), 1) // group


def block_ones(rows, row_group, cols, col_group):
    r = lax.broadcasted_iota(jnp.int32, (rows, cols), 0) // row_group
    return (r == lane_group(rows, cols, col_group)).astype(F32).astype(BF16)


def put(buf, rows, x):
    cols = x.shape[1]
    if cols < 128:
        x = jnp.concatenate([x] * (128 // cols), axis=1)
    for c in range(buf.shape[0]):
        buf[c, rows, :] = x[:, c * 128 : (c + 1) * 128]


def get(buf, rows, cols):
    x = jnp.concatenate([buf[c, rows, :] for c in range(buf.shape[0])], axis=1)
    return x[:, :cols]


def own_head(parts, group):
    rows, cols = parts[0].shape
    if len(parts) == 1:
        return parts[0]
    lanes = lane_group(rows, cols, group)
    total = jnp.where(lanes == 0, parts[0], 0.0)
    for h in range(1, len(parts)):
        total = jnp.where(lanes == h, parts[h], total)
    return total


def commit_kernel(steps, heads, acum_ref, k_ref, v_ref, a_ref, b_ref, s_ref, out_ref, kbuf, pbuf, ubuf):
    seqs, cols, width = s_ref.shape
    group = cols // heads
    rows = steps * heads
    kbuf[...] = k_ref[...].astype(F32)
    for s in range(seqs):
        put(
            pbuf,
            pl.ds(s * rows, rows),
            dot_nt(k_ref[pl.ds(s * rows, rows), :], s_ref[s].astype(BF16)),
        )
    keys = [
        [kbuf[pl.ds(t * heads + h, seqs, stride=rows), :] for h in range(heads)] for t in range(steps)
    ]
    pairs = [(i, t) for t in range(steps) for i in range(t + 1)]
    products = [
        jnp.concatenate([keys[i][h] * keys[t][h] for h in range(heads)], axis=1) for i, t in pairs
    ]
    sums = jnp.dot(
        jnp.concatenate(products, axis=0).astype(BF16),
        block_ones(heads * width, width, cols, group),
        preferred_element_type=F32,
    )
    gram = {pair: sums[n * seqs : (n + 1) * seqs] for n, pair in enumerate(pairs)}
    norm = [lax.rsqrt(gram[(t, t)] + EPS) for t in range(steps)]
    decay = [a_ref[t] for t in range(steps)]
    fed = []
    through = None
    for t in range(steps):
        seen = own_head(
            [get(pbuf, pl.ds(t * heads + h, seqs, stride=rows), cols) for h in range(heads)], group
        )
        through = decay[t] if through is None else through * decay[t]
        fed = [decay[t] * f for f in fed]
        predicted = through * seen
        for i in range(t):
            predicted = predicted + gram[(i, t)] * fed[i]
        fed.append(b_ref[t] * (v_ref[t] - norm[t] * predicted) * norm[t])
    lanes = lane_group(seqs, cols, group)
    for t in range(steps):
        for h in range(heads):
            put(ubuf, pl.ds(t * heads + h, seqs, stride=rows), jnp.where(lanes == h, fed[t], 0.0))
    base = pl.program_id(0) * seqs
    for s in range(seqs):
        update = lax.dot_general(
            get(ubuf, pl.ds(s * rows, rows), cols).astype(BF16),
            k_ref[pl.ds(s * rows, rows), :],
            TN,
            preferred_element_type=F32,
        )
        for h in range(heads):
            span = slice(h * group, (h + 1) * group)
            out_ref[s, span, :] = acum_ref[(base + s) * heads + h] * s_ref[s, span, :] + update[span]


def commit(state, prev_keys, prev_values, retain, beta):
    seqs, steps, heads, width = prev_keys.shape
    group = state.shape[2]
    cols = heads * group
    block = 8
    rows = steps * heads

    def wide(x):
        x = jnp.transpose(x, (1, 0, 2))[..., None]
        return jnp.broadcast_to(x, (steps, seqs, heads, group)).reshape(steps, seqs, cols)

    values = jnp.transpose(prev_values, (1, 0, 2, 3)).astype(F32).reshape(steps, seqs, cols)
    acum = jnp.prod(retain, axis=1).reshape(-1)
    coef = pl.BlockSpec((steps, block, cols), lambda i: (0, i, 0))
    big = pl.BlockSpec((block, cols, width), lambda i: (i, 0, 0))
    return pl.pallas_call(
        functools.partial(commit_kernel, steps, heads),
        grid=(seqs // block,),
        out_shape=jax.ShapeDtypeStruct((seqs, cols, width), F32),
        in_specs=[
            pl.BlockSpec(memory_space=pltpu.SMEM),
            pl.BlockSpec((block * rows, width), lambda i: (i, 0)),
            coef,
            coef,
            coef,
            big,
        ],
        out_specs=big,
        scratch_shapes=[
            pltpu.VMEM((block * rows, width), F32),
            pltpu.VMEM((pl.cdiv(cols, 128), block * rows, 128), F32),
            pltpu.VMEM((pl.cdiv(cols, 128), block * rows, 128), F32),
        ],
    )(
        acum,
        prev_keys.reshape(seqs * rows, width),
        values,
        wide(retain),
        wide(beta),
        state.reshape(seqs, cols, width),
    )


def verify_kernel(
    nkv, heads, steps,
    tok_ref, gain_ref, wq_ref, wk_ref, wv_ref, wg_ref, wd_ref, wb_ref, rate_ref, hg_ref, wo_ref, st_ref,
    out_ref,
    xs, w, wo, st, acc, halves, kbuf, pbuf, ssend, srecv, psend, precv, part, zsend, zrecv,
    w_sem, big_sem, ag_send, ag_recv, fw_send, ex_send, ex_recv, p_send, p_recv, z_send, z_recv,
):
    kv, tp = lax.axis_index("kv"), lax.axis_index("tp")
    rows, feat = tok_ref.shape
    seqs, cols, width = st.shape
    group = cols // heads
    allheads = wd_ref.shape[0]
    partner = {"tp": 1 - tp}

    def far(d):
        return lax.rem(kv + d, nkv)

    hops = sorted(range(1, nkv), key=lambda d: (min(d, nkv - d), d))
    order = [(0, 0), (0, 1)] + [(d, e) for d in hops for e in (0, 1)]

    def owner(d, e):
        return far(d) * 2 + (tp if e == 0 else 1 - tp)

    def span(block):
        return pl.ds(pl.multiple_of(block * feat, 128), feat)

    mats = (wq_ref, wk_ref, wv_ref, wg_ref, wd_ref, wb_ref)
    tops = [0, cols, 2 * cols, 3 * cols, 4 * cols, 4 * cols + allheads]
    loads = []
    for n, (d, e) in enumerate(order):
        there = span(owner(d, e))
        chunk = []
        for m, ref in enumerate(mats):
            chunk.append(
                pltpu.make_async_copy(
                    ref.at[:, there], w.at[pl.ds(tops[m], ref.shape[0]), there], w_sem.at[n, m]
                )
            )
        loads.append(chunk)

    barrier = pltpu.get_barrier_semaphore()
    pl.semaphore_signal(barrier, inc=1, device_id=partner, device_id_type=MESH)
    for d in hops:
        pl.semaphore_signal(barrier, inc=1, device_id={"kv": far(d)}, device_id_type=MESH)
    for chunk in loads:
        for copy in chunk:
            copy.start()
    st_copy = pltpu.make_async_copy(st_ref, st, big_sem.at[0])
    wo_copy = pltpu.make_async_copy(wo_ref, wo, big_sem.at[1])
    st_copy.start()
    wo_copy.start()
    pl.semaphore_wait(barrier, nkv)

    def remote(src, dst, send, recv, where):
        return pltpu.make_async_remote_copy(
            src_ref=src, dst_ref=dst, send_sem=send, recv_sem=recv, device_id=where, device_id_type=MESH
        )

    mine = owner(0, 0)
    pending = []
    for d in hops:
        copy = remote(tok_ref, xs.at[mine], ag_send.at[d], ag_recv.at[mine], {"kv": far(d)})
        copy.start()
        pending.append(copy)
    copy = remote(tok_ref, xs.at[mine], ag_send.at[0], ag_recv.at[mine], partner)
    copy.start()
    pending.append(copy)

    square = jnp.zeros((rows, 1), F32)
    for n, (d, e) in enumerate(order):
        block = owner(d, e)
        if n == 0:
            x = tok_ref[...]
        else:
            remote(tok_ref, xs.at[block], ag_send.at[0], ag_recv.at[block], partner).wait_recv()
            if e == 0:
                copy = remote(xs.at[block], xs.at[block], fw_send.at[d], ag_recv.at[block], partner)
                copy.start()
                pending.append(copy)
            x = xs[block]
        x = x.astype(F32)
        square = square + jnp.sum(x * x, axis=1, keepdims=True)
        xg = (x * gain_ref[:, span(block)]).astype(BF16)
        for copy in loads[n]:
            copy.wait()
        product = dot_nt(xg, w[:, span(block)])
        if n == 0:
            acc[...] = product
        else:
            acc[...] += product
    scale = lax.rsqrt(square / (feat * nkv * 2) + EPS)

    halves[tp] = (acc[:, : 2 * cols] * scale).astype(BF16)
    qk = remote(halves.at[tp], halves.at[tp], ex_send.at[0], ex_recv.at[0], partner)
    qk.start()
    pending_tail = [qk]

    value = silu((acc[:, 2 * cols : 3 * cols] * scale).astype(BF16).astype(F32))
    gate = silu((acc[:, 3 * cols : 4 * cols] * scale).astype(BF16).astype(F32)) * hg_ref[...]
    pre = acc[:, 4 * cols :] * scale
    pick_row = lax.broadcasted_iota(jnp.int32, (allheads, cols), 0)
    pick = (pick_row == kv * heads + lane_group(allheads, cols, group)).astype(F32)
    dec = jnp.dot(pre[:, :allheads], pick, precision=lax.Precision.HIGHEST, preferred_element_type=F32)
    bet = jnp.dot(pre[:, allheads:], pick, precision=lax.Precision.HIGHEST, preferred_element_type=F32)
    soft = jnp.maximum(dec, 0.0) + jnp.log1p(jnp.exp(-jnp.abs(dec)))
    retain = jnp.exp(-(rate_ref[...] * soft))
    strength = jax.nn.sigmoid(bet)
    ones_wide = block_ones(heads * width, width, cols, group)
    ones_cols = block_ones(cols, group, cols, group)

    def at(x, t):
        return x[t * seqs : (t + 1) * seqs]

    remote(halves.at[1 - tp], halves.at[1 - tp], ex_send.at[0], ex_recv.at[0], partner).wait_recv()
    low, high = halves[0].astype(F32), halves[1].astype(F32)
    low, high = silu(low), silu(high)

    def whole(kind):
        base = kind * cols
        pieces = []
        for h in range(heads):
            lanes = slice(base + h * group, base + (h + 1) * group)
            pieces += [low[:, lanes], high[:, lanes]]
        return jnp.concatenate(pieces, axis=1)

    query, key = whole(0), whole(1)
    for t in range(steps):
        for h in range(heads):
            lanes = slice(h * width, (h + 1) * width)
            place = (h * 2) * steps + t
            kbuf[pl.ds(place, seqs, stride=heads * 2 * steps), :] = at(key, t)[:, lanes]
            kbuf[pl.ds(place + steps, seqs, stride=heads * 2 * steps), :] = at(query, t)[:, lanes]
    st_copy.wait()
    tall = 2 * steps
    for s in range(seqs):
        stacked = kbuf[pl.ds(s * heads * tall, heads * tall), :].astype(BF16)
        seen = dot_nt(stacked, st[s].astype(BF16))
        put(
            pbuf,
            pl.ds(s * tall, tall),
            own_head([seen[h * tall : (h + 1) * tall] for h in range(heads)], group),
        )
    pairs = [("k", i, t) for t in range(steps) for i in range(t + 1)]
    pairs += [("q", i, t) for t in range(steps) for i in range(t + 1)]
    products = [at(key, i) * at(key if kind == "k" else query, t) for kind, i, t in pairs]
    products.append(query * query)
    sums = jnp.dot(
        jnp.concatenate(products, axis=0).astype(BF16), ones_wide, preferred_element_type=F32
    )
    gram = {pair: at(sums, n) for n, pair in enumerate(pairs)}
    qsq = sums[len(pairs) * seqs :]
    qnorm = lax.rsqrt(qsq + EPS) * width ** (-0.5)
    fed, through, outs = [], None, []
    for t in range(steps):
        norm = lax.rsqrt(gram[("k", t, t)] + EPS)
        a = at(retain, t)
        through = a if through is None else through * a
        fed = [a * f for f in fed]
        predicted = through * get(pbuf, pl.ds(t, seqs, stride=tall), cols)
        for i in range(t):
            predicted = predicted + gram[("k", i, t)] * fed[i]
        fed.append(at(strength, t) * (at(value, t) - norm * predicted) * norm)
        o = through * get(pbuf, pl.ds(steps + t, seqs, stride=tall), cols)
        for i in range(t + 1):
            o = o + gram[("q", i, t)] * fed[i]
        outs.append(o * at(qnorm, t))
    heads_out = jnp.concatenate(outs, axis=0)
    squares = jnp.dot((heads_out * heads_out).astype(BF16), ones_cols, preferred_element_type=F32)
    ssend[...] = squares
    sq = remote(ssend, srecv, ex_send.at[1], ex_recv.at[1], partner)
    sq.start()
    ready = heads_out * gate
    wo_copy.wait()
    sq.wait_recv()
    pending_tail.append(sq)
    total = squares + srecv[...]
    scaled = (ready * lax.rsqrt(total / (2 * group) + EPS)).astype(BF16)

    targets = sorted(range(1, nkv), key=lambda d: (-min(d, nkv - d), d)) + [0]
    crossing = []
    for j, d in enumerate(targets):
        psend[j] = jnp.dot(scaled, wo[:, span(owner(d, 1))], preferred_element_type=F32).astype(BF16)
        copy = remote(psend.at[j], precv.at[j], p_send.at[j], p_recv.at[j], partner)
        copy.start()
        crossing.append(copy)
        part[j] = jnp.dot(scaled, wo[:, span(owner(d, 0))], preferred_element_type=F32)
    flights = []
    for j, d in enumerate(targets):
        crossing[j].wait_recv()
        both = part[j] + precv[j].astype(F32)
        if d:
            zsend[j] = both.astype(BF16)
            copy = remote(zsend.at[j], zrecv.at[j], z_send.at[j], z_recv.at[j], {"kv": far(d)})
            copy.start()
            flights.append(copy)
    mixed = both
    for j, copy in sorted(enumerate(flights), key=lambda f: -f[0]):
        copy.wait_recv()
        mixed = mixed + zrecv[j].astype(F32)
    out_ref[...] = mixed.astype(BF16)
    for copy in pending + pending_tail + crossing + flights:
        copy.wait_send()


def local(
    nkv,
    tokens,
    norm_gain,
    w_query,
    w_key,
    w_value,
    w_gate,
    w_decay,
    w_beta,
    decay_rate,
    head_gain,
    w_out,
    state,
    prev_keys,
    prev_values,
    prev_decay,
    prev_beta,
    accepted,
):
    seqs, steps, feat = tokens.shape
    heads, group, width = state.shape[1:]
    cols = heads * group
    rows = seqs * steps
    full = norm_gain.shape[0]
    allheads = w_decay.shape[1]
    mask = (jnp.arange(steps)[None, :] < accepted[:, None]).astype(F32)[:, :, None]
    committed = commit(state, prev_keys, prev_values, jnp.exp(-prev_decay * mask), prev_beta * mask)

    vmem = pl.BlockSpec(memory_space=pltpu.VMEM)
    hbm = pl.BlockSpec(memory_space=pl.ANY)
    blocks = 2 * nkv
    tall = 2 * steps
    DMA = pltpu.SemaphoreType.DMA
    mixed = pl.pallas_call(
        functools.partial(verify_kernel, nkv, heads, steps),
        out_shape=jax.ShapeDtypeStruct((rows, feat), BF16),
        in_specs=[vmem, vmem] + [hbm] * 6 + [vmem, vmem] + [hbm] * 2,
        out_specs=vmem,
        scratch_shapes=[
            pltpu.VMEM((blocks, rows, feat), BF16),
            pltpu.VMEM((4 * cols + 2 * allheads, full), BF16),
            pltpu.VMEM((cols, full), BF16),
            pltpu.VMEM((seqs, cols, width), F32),
            pltpu.VMEM((rows, 4 * cols + 2 * allheads), F32),
            pltpu.VMEM((2, rows, 2 * cols), BF16),
            pltpu.VMEM((seqs * heads * tall, width), F32),
            pltpu.VMEM((pl.cdiv(cols, 128), seqs * tall, 128), F32),
            pltpu.VMEM((rows, cols), F32),
            pltpu.VMEM((rows, cols), F32),
            pltpu.VMEM((nkv, rows, feat), BF16),
            pltpu.VMEM((nkv, rows, feat), BF16),
            pltpu.VMEM((nkv, rows, feat), F32),
            pltpu.VMEM((nkv, rows, feat), BF16),
            pltpu.VMEM((nkv, rows, feat), BF16),
            DMA((blocks, 6)),
            DMA((2,)),
            DMA((nkv,)),
            DMA((blocks,)),
            DMA((nkv,)),
            DMA((2,)),
            DMA((2,)),
            DMA((nkv,)),
            DMA((nkv,)),
            DMA((nkv,)),
            DMA((nkv,)),
        ],
        compiler_params=pltpu.CompilerParams(
            collective_id=0, has_side_effects=True, vmem_limit_bytes=60 * 1024 * 1024
        ),
    )(
        jnp.transpose(tokens, (1, 0, 2)).reshape(rows, feat),
        norm_gain.reshape(1, full),
        w_query.reshape(cols, full),
        w_key.reshape(cols, full),
        w_value.reshape(cols, full),
        w_gate.reshape(cols, full),
        w_decay.T,
        w_beta.T,
        jnp.repeat(decay_rate, group).reshape(1, cols),
        jnp.tile(head_gain, heads).reshape(1, cols),
        w_out.reshape(cols, full),
        committed,
    )
    mixed = jnp.transpose(mixed.reshape(steps, seqs, feat), (1, 0, 2))
    return mixed, committed.reshape(state.shape)


def solution(mesh):
    in_specs = (
        P(("grp", "dp"), None, ("kv", "tp")),
        P(),
        P("kv", "tp", None),
        P("kv", "tp", None),
        P("kv", "tp", None),
        P("kv", "tp", None),
        P(),
        P(),
        P("kv"),
        P("tp"),
        P("kv", "tp", None),
        P(("grp", "dp"), "kv", "tp", None),
        P(("grp", "dp"), None, "kv", None),
        P(("grp", "dp"), None, "kv", "tp"),
        P(("grp", "dp"), None, "kv"),
        P(("grp", "dp"), None, "kv"),
        P(("grp", "dp")),
    )
    out_specs = (P(("grp", "dp"), None, ("kv", "tp")), P(("grp", "dp"), "kv", "tp", None))
    return jax.shard_map(
        functools.partial(local, mesh.shape["kv"]),
        mesh=mesh, in_specs=in_specs, out_specs=out_specs, check_vma=False,
    )
```

profile of v0, /device:TPU:0, one launch (start us, length us, event | category | flops | bytes accessed | tf_op | source)
XLA Modules:
  0.0 49.0 jit_solution(8439130017007024949)
XLA Ops:
  0.6 0.7 %fusion.2 = f32[24,4]{0,1:T(4,128)S(1)} fusion(s32[24]{0:T(128)} %param.33), kind=kLoop, calls=%fused_computation.7 | loop fusion | flops 192 | bytes 480 | tf_op jit(solution)/shard_map/convert_element_type | solution.py:387
  1.3 0.7 %fusion = (f32[4,24,4]{1,2,0:T(4,128)S(1)}, f32[24,4]{0,1:T(4,128)S(1)}, f32[4,24,4]{1,2,0:T(4,128)S(1)}) fusion(f32[24,4,4]{0,2,1:T(4,128)} %param.31, f32[24,4]{0,1:T(4,128)S(1)} %fusion.2, f32[24,4,4]{0,2,1:T(4,128)} %param.32), kind=kLoop, calls=%fused_computation.4 | loop fusion | flops 1440 | bytes 6912 | tf_op jit(solution)/shard_map/transpose | solution.py:122
  2.0 0.1 copy.32
  2.1 0.2 broadcast_in_dim.7
  2.3 0.8 %reshape.87.a_ref = f32[4,24,256]{2,1,0:T(8,128)} reshape(f32[4,24,4,64]{3,2,1,0:T(4,128)S(1)} %broadcast_in_dim.7) | data formatting | bytes 196608 | tf_op jit(solution)/shard_map/reshape | solution.py:123
  3.1 0.1 copy.33
  3.2 0.2 broadcast_in_dim.8
  3.4 0.8 %reshape.88.b_ref = f32[4,24,256]{2,1,0:T(8,128)} reshape(f32[4,24,4,64]{3,2,1,0:T(4,128)S(1)} %broadcast_in_dim.8) | data formatting | bytes 196608 | tf_op jit(solution)/shard_map/reshape | solution.py:123
  4.2 0.1 copy.30
  4.2 0.6 %reshape.83.acum_ref = f32[96]{0:T(128)} reshape(f32[24,4]{1,0:T(8,128)S(1)} %copy.30) | data formatting | bytes 768 | tf_op jit(solution)/shard_map/reshape | solution.py:126
  4.9 0.9 %convert_bitcast_fusion = f32[4,24,4,64]{3,2,0,1:T(4,128)S(1)} fusion(bf16[24,4,4,64]{3,2,1,0:T(4,128)(2,1)} %param.30), kind=kLoop, calls=%fused_computation | loop fusion | flops 24576 | bytes 147456 | tf_op jit(solution)/shard_map/reshape | solution.py:125
  5.8 0.1 reshape.95
  5.9 0.7 %copy.35.v_ref = f32[4,24,256]{2,1,0:T(8,128)} copy(f32[4,24,256]{2,0,1:T(4,128)S(1)} %reshape.95) | data formatting | bytes 196608 | tf_op jit(solution)/shard_map/reshape | solution.py:125
  6.6 0.0 copy-start
  6.6 0.0 copy-start.1
  6.6 0.0 copy-start.2
  6.6 5.5 %shard_map.176.st_ref = f32[24,256,128]{2,1,0:T(8,128)} custom-call(f32[96]{0:T(128)} %reshape.83.acum_ref, bf16[384,128]{1,0:T(8,128)(2,1)} %bitcast.38, f32[4,24,256]{2,1,0:T(8,128)} %copy.35.v_ref, f32[4,24,256]{2,1,0:T(8,128)} %reshape.87.a_ref, f32[4,24,256]{2,1,0:T(8,128)} %reshape.88.b_ref, f32[24,256,128]{2,1,0:T(8,128)} %bitcast.26), custom_call_target="tpu_custom_call" | custom-call | tf_op jit(solution)/shard_map/pallas_call | solution.py:129
  12.1 0.0 copy-done
  12.1 0.7 %copy.29 = bf16[4,24,512]{2,1,0:T(8,128)(2,1)} copy(bf16[4,24,512]{2,0,1:T(4,128)(2,1)S(1)} %bitcast.36) | data formatting | bytes 196608 | tf_op jit(solution)/shard_map/transpose | solution.py:432
  12.7 0.0 copy-done.1
  12.7 0.1 broadcast_in_dim.6
  12.8 0.7 %reshape_reshape.3.rate_ref = f32[1,256]{1,0:T(1,128)} reshape(f32[4,64]{1,0:T(4,128)S(1)} %broadcast_in_dim.6) | data formatting | bytes 2048 | tf_op jit(solution)/shard_map/reshape;reshape | solution.py:440
  13.5 0.0 copy-done.2
  13.5 0.7 %reshape_tile.3.hg_ref = f32[1,256]{1,0:T(1,128)} reshape(f32[4,64]{1,0:T(4,128)S(1)} %tile.2) | data formatting | bytes 2048 | tf_op jit(solution)/shard_map/reshape;tile | solution.py:441
  14.1 33.2 %shard_map.177 = bf16[96,512]{1,0:T(8,128)(2,1)} custom-call(bf16[96,512]{1,0:T(8,128)(2,1)} %bitcast.32, f32[1,4096]{1,0:T(1,128)} %bitcast.39, bf16[256,4096]{1,0:T(8,128)(2,1)} %bitcast.27, bf16[256,4096]{1,0:T(8,128)(2,1)} %bitcast.28, bf16[256,4096]{1,0:T(8,128)(2,1)} %bitcast.29, bf16[256,4096]{1,0:T(8,128)(2,1)} %bitcast.30, ...), custom_call_target="tpu_custom_call" | custom-call | tf_op jit(solution)/shard_map/pallas_call | solution.py:395
  47.4 1.6 %copy.37 = bf16[4,24,512]{2,0,1:T(4,128)(2,1)} copy(bf16[4,24,512]{2,1,0:T(8,128)(2,1)} %bitcast.33) | data formatting | bytes 196608 | tf_op jit(solution)/shard_map/reshape | solution.py:445
  (1 shorter events, 0.0 us)
Async XLA Ops:
  6.6 5.5 %copy-start = (bf16[24,4,512]{2,1,0:T(4,128)(2,1)S(1)}, bf16[24,4,512]{2,1,0:T(4,128)(2,1)}, u32[]{:S(2)}) copy-start(bf16[24,4,512]{2,1,0:T(4,128)(2,1)} %param.17) | copy-start | bytes 294916
  6.6 6.2 %copy-start.1 = (f32[4]{0:T(128)S(1)}, f32[4]{0:T(128)}, u32[]{:S(2)}) copy-start(f32[4]{0:T(128)} %param.25) | copy-start | bytes 52
  6.6 6.9 %copy-start.2 = (f32[64]{0:T(128)S(1)}, f32[64]{0:T(128)}, u32[]{:S(2)}) copy-start(f32[64]{0:T(128)} %param.26) | copy-start | bytes 772
where the time goes:
time: 49.3 us; the launch traced here: 49 us
  Pallas kernels  38.7 us (78%)
  local copies, waits for them, and re-layouts  7.26 us (15%)
  other arithmetic  2.3 us (5%)
  between operations  0.67 us (1%)
    pallas_call x1, Pallas kernels, local(): pl.pallas_call(functools.partial(verify_kernel, nkv, heads, steps), out_s...  33.2 us
    pallas_call x1, Pallas kernels, commit(): pl.pallas_call(functools.partial(commit_kernel, steps, heads), grid=(seqs...  5.51 us
    reshape x2, local copies, waits for them, and re-layouts, wide(): jnp.broadcast_to(x, (steps, seqs, heads, group)).reshape(steps, seqs, cols)  1.6 us
    reshape x1, local copies, waits for them, and re-layouts, local(): mixed = jnp.transpose(mixed.reshape(steps, seqs, feat), (1, 0, 2))  1.58 us

commit v1 on v0

--- a/solution.py
+++ b/solution.py
@@ -56,20 +56,40 @@
     return total
 
 
-def commit_kernel(steps, heads, acum_ref, k_ref, v_ref, a_ref, b_ref, s_ref, out_ref, kbuf, pbuf, ubuf):
+def commit_kernel(steps, heads, k_ref, v_ref, pd_ref, pb_ref, acc_ref, s_ref, out_ref, kbuf, vbuf, pbuf, ubuf, coef):
     seqs, cols, width = s_ref.shape
     group = cols // heads
     rows = steps * heads
+    total = acc_ref.shape[1]
+
+    @pl.when(pl.program_id(0) == 0)
+    def _():
+        step_of = lax.broadcasted_iota(jnp.int32, (rows, total), 0) // heads
+        mask = (step_of < acc_ref[...]).astype(F32)
+        retain = jnp.exp(-pd_ref[...] * mask)
+        beta = pb_ref[...] * mask
+        head_of = lax.broadcasted_iota(jnp.int32, (rows, cols), 0)
+        for t in range(steps):
+            pick = (head_of == t * heads + lane_group(rows, cols, group)).astype(F32)
+            for n, x in enumerate((retain, beta)):
+                coef[n * steps + t] = lax.dot_general(
+                    x, pick, TN, precision=lax.Precision.HIGHEST, preferred_element_type=F32
+                )
+
     kbuf[...] = k_ref[...].astype(F32)
+    values = v_ref[...].astype(F32)
+    vbuf[...] = jnp.concatenate([values] * (width // group), axis=1)
     for s in range(seqs):
         put(
             pbuf,
             pl.ds(s * rows, rows),
             dot_nt(k_ref[pl.ds(s * rows, rows), :], s_ref[s].astype(BF16)),
         )
-    keys = [
-        [kbuf[pl.ds(t * heads + h, seqs, stride=rows), :] for h in range(heads)] for t in range(steps)
-    ]
+
+    def every(t, h):
+        return pl.ds(t * heads + h, seqs, stride=rows)
+
+    keys = [[kbuf[every(t, h), :] for h in range(heads)] for t in range(steps)]
     pairs = [(i, t) for t in range(steps) for i in range(t + 1)]
     products = [
         jnp.concatenate([keys[i][h] * keys[t][h] for h in range(heads)], axis=1) for i, t in pairs
@@ -81,24 +101,27 @@
     )
     gram = {pair: sums[n * seqs : (n + 1) * seqs] for n, pair in enumerate(pairs)}
     norm = [lax.rsqrt(gram[(t, t)] + EPS) for t in range(steps)]
-    decay = [a_ref[t] for t in range(steps)]
+    here = pl.ds(pl.multiple_of(pl.program_id(0) * seqs, seqs), seqs)
     fed = []
     through = None
+    copies = max(1, cols // width)
     for t in range(steps):
-        seen = own_head(
-            [get(pbuf, pl.ds(t * heads + h, seqs, stride=rows), cols) for h in range(heads)], group
+        decay = coef[t, here, :]
+        seen = own_head([get(pbuf, every(t, h), cols) for h in range(heads)], group)
+        value = own_head(
+            [jnp.concatenate([vbuf[every(t, h), :]] * copies, axis=1)[:, :cols] for h in range(heads)],
+            group,
         )
-        through = decay[t] if through is None else through * decay[t]
-        fed = [decay[t] * f for f in fed]
+        through = decay if through is None else through * decay
+        fed = [decay * f for f in fed]
         predicted = through * seen
         for i in range(t):
             predicted = predicted + gram[(i, t)] * fed[i]
-        fed.append(b_ref[t] * (v_ref[t] - norm[t] * predicted) * norm[t])
+        fed.append(coef[steps + t, here, :] * (value - norm[t] * predicted) * norm[t])
     lanes = lane_group(seqs, cols, group)
     for t in range(steps):
         for h in range(heads):
-            put(ubuf, pl.ds(t * heads + h, seqs, stride=rows), jnp.where(lanes == h, fed[t], 0.0))
-    base = pl.program_id(0) * seqs
+            put(ubuf, every(t, h), jnp.where(lanes == h, fed[t], 0.0))
     for s in range(seqs):
         update = lax.dot_general(
             get(ubuf, pl.ds(s * rows, rows), cols).astype(BF16),
@@ -108,61 +131,68 @@
         )
         for h in range(heads):
             span = slice(h * group, (h + 1) * group)
-            out_ref[s, span, :] = acum_ref[(base + s) * heads + h] * s_ref[s, span, :] + update[span]
-
-
-def commit(state, prev_keys, prev_values, retain, beta):
+            kept = through[s : s + 1, h * group : h * group + 1]
+            out_ref[s, span, :] = kept * s_ref[s, span, :] + update[span]
+
+
+def commit(state, prev_keys, prev_values, prev_decay, prev_beta, accepted):
     seqs, steps, heads, width = prev_keys.shape
     group = state.shape[2]
     cols = heads * group
     block = 8
     rows = steps * heads
-
-    def wide(x):
-        x = jnp.transpose(x, (1, 0, 2))[..., None]
-        return jnp.broadcast_to(x, (steps, seqs, heads, group)).reshape(steps, seqs, cols)
-
-    values = jnp.transpose(prev_values, (1, 0, 2, 3)).astype(F32).reshape(steps, seqs, cols)
-    acum = jnp.prod(retain, axis=1).reshape(-1)
-    coef = pl.BlockSpec((steps, block, cols), lambda i: (0, i, 0))
     big = pl.BlockSpec((block, cols, width), lambda i: (i, 0, 0))
+    coef = pl.BlockSpec((rows, seqs), lambda i: (0, 0))
+    tiles = pl.cdiv(cols, 128)
     return pl.pallas_call(
         functools.partial(commit_kernel, steps, heads),
         grid=(seqs // block,),
         out_shape=jax.ShapeDtypeStruct((seqs, cols, width), F32),
         in_specs=[
-            pl.BlockSpec(memory_space=pltpu.SMEM),
             pl.BlockSpec((block * rows, width), lambda i: (i, 0)),
+            pl.BlockSpec((block * rows, group), lambda i: (i, 0)),
             coef,
             coef,
-            coef,
+            pl.BlockSpec((1, seqs), lambda i: (0, 0)),
             big,
         ],
         out_specs=big,
         scratch_shapes=[
             pltpu.VMEM((block * rows, width), F32),
-            pltpu.VMEM((pl.cdiv(cols, 128), block * rows, 128), F32),
-            pltpu.VMEM((pl.cdiv(cols, 128), block * rows, 128), F32),
+            pltpu.VMEM((block * rows, width), F32),
+            pltpu.VMEM((tiles, block * rows, 128), F32),
+            pltpu.VMEM((tiles, block * rows, 128), F32),
+            pltpu.VMEM((2 * steps, seqs, cols), F32),
         ],
+        cost_estimate=pl.CostEstimate(
+            flops=4 * seqs * rows * cols * width, bytes_accessed=8 * state.size, transcendentals=0
+        ),
     )(
-        acum,
         prev_keys.reshape(seqs * rows, width),
-        values,
-        wide(retain),
-        wide(beta),
+        prev_values.reshape(seqs * rows, group),
+        jnp.transpose(prev_decay, (1, 2, 0)).reshape(rows, seqs),
+        jnp.transpose(prev_beta, (1, 2, 0)).reshape(rows, seqs),
+        accepted.reshape(1, seqs),
         state.reshape(seqs, cols, width),
     )
 
 
 def verify_kernel(
+    nkv, heads, steps, tok_ref, *refs
+):
+    got, refs = refs[: nkv - 1], refs[nkv - 1 :]
+    verify(nkv, heads, steps, (tok_ref, *got), *refs)
+
+
+def verify(
     nkv, heads, steps,
-    tok_ref, gain_ref, wq_ref, wk_ref, wv_ref, wg_ref, wd_ref, wb_ref, rate_ref, hg_ref, wo_ref, st_ref,
+    got, gain_ref, wq_ref, wk_ref, wv_ref, wg_ref, wd_ref, wb_ref, rate_ref, hg_ref, wo_ref, st_ref,
     out_ref,
     xs, w, wo, st, acc, halves, kbuf, pbuf, ssend, srecv, psend, precv, part, zsend, zrecv,
-    w_sem, big_sem, ag_send, ag_recv, fw_send, ex_send, ex_recv, p_send, p_recv, z_send, z_recv,
+    w_sem, big_sem, ag_send, ag_recv, ex_send, ex_recv, p_send, p_recv, z_send, z_recv,
 ):
     kv, tp = lax.axis_index("kv"), lax.axis_index("tp")
-    rows, feat = tok_ref.shape
+    rows, feat = got[0].shape
     seqs, cols, width = st.shape
     group = cols // heads
     allheads = wd_ref.shape[0]
@@ -172,7 +202,7 @@
         return lax.rem(kv + d, nkv)
 
     hops = sorted(range(1, nkv), key=lambda d: (min(d, nkv - d), d))
-    order = [(0, 0), (0, 1)] + [(d, e) for d in hops for e in (0, 1)]
+    order = [(d, e) for e in (0, 1) for d in [0] + hops]
 
     def owner(d, e):
         return far(d) * 2 + (tp if e == 0 else 1 - tp)
@@ -212,28 +242,20 @@
             src_ref=src, dst_ref=dst, send_sem=send, recv_sem=recv, device_id=where, device_id_type=MESH
         )
 
-    mine = owner(0, 0)
     pending = []
-    for d in hops:
-        copy = remote(tok_ref, xs.at[mine], ag_send.at[d], ag_recv.at[mine], {"kv": far(d)})
+    for d in [0] + hops:
+        copy = remote(got[d], xs.at[d], ag_send.at[d], ag_recv.at[d], partner)
         copy.start()
         pending.append(copy)
-    copy = remote(tok_ref, xs.at[mine], ag_send.at[0], ag_recv.at[mine], partner)
-    copy.start()
-    pending.append(copy)
 
     square = jnp.zeros((rows, 1), F32)
     for n, (d, e) in enumerate(order):
         block = owner(d, e)
-        if n == 0:
-            x = tok_ref[...]
+        if e == 0:
+            x = got[d][...]
         else:
-            remote(tok_ref, xs.at[block], ag_send.at[0], ag_recv.at[block], partner).wait_recv()
-            if e == 0:
-                copy = remote(xs.at[block], xs.at[block], fw_send.at[d], ag_recv.at[block], partner)
-                copy.start()
-                pending.append(copy)
-            x = xs[block]
+            pending[[0, *hops].index(d)].wait_recv()
+            x = xs[d]
         x = x.astype(F32)
         square = square + jnp.sum(x * x, axis=1, keepdims=True)
         xg = (x * gain_ref[:, span(block)]).astype(BF16)
@@ -252,14 +274,18 @@
     pending_tail = [qk]
 
     value = silu((acc[:, 2 * cols : 3 * cols] * scale).astype(BF16).astype(F32))
-    gate = silu((acc[:, 3 * cols : 4 * cols] * scale).astype(BF16).astype(F32)) * hg_ref[...]
+    gate = silu((acc[:, 3 * cols : 4 * cols] * scale).astype(BF16).astype(F32)) * jnp.concatenate([hg_ref[...]] * heads, axis=1)
     pre = acc[:, 4 * cols :] * scale
     pick_row = lax.broadcasted_iota(jnp.int32, (allheads, cols), 0)
     pick = (pick_row == kv * heads + lane_group(allheads, cols, group)).astype(F32)
     dec = jnp.dot(pre[:, :allheads], pick, precision=lax.Precision.HIGHEST, preferred_element_type=F32)
     bet = jnp.dot(pre[:, allheads:], pick, precision=lax.Precision.HIGHEST, preferred_element_type=F32)
+    lanes_own = lane_group(1, cols, group)
+    rate = jnp.zeros((1, cols), F32)
+    for h in range(heads):
+        rate = jnp.where(lanes_own == h, rate_ref[:, h : h + 1], rate)
     soft = jnp.maximum(dec, 0.0) + jnp.log1p(jnp.exp(-jnp.abs(dec)))
-    retain = jnp.exp(-(rate_ref[...] * soft))
+    retain = jnp.exp(-(rate * soft))
     strength = jax.nn.sigmoid(bet)
     ones_wide = block_ones(heads * width, width, cols, group)
     ones_cols = block_ones(cols, group, cols, group)
@@ -384,8 +410,11 @@
     rows = seqs * steps
     full = norm_gain.shape[0]
     allheads = w_decay.shape[1]
-    mask = (jnp.arange(steps)[None, :] < accepted[:, None]).astype(F32)[:, :, None]
-    committed = commit(state, prev_keys, prev_values, jnp.exp(-prev_decay * mask), prev_beta * mask)
+    flat = jnp.transpose(tokens, (1, 0, 2)).reshape(rows, feat)
+    got = [
+        lax.ppermute(flat, "kv", [((i + d) % nkv, i) for i in range(nkv)]) for d in range(1, nkv)
+    ]
+    committed = commit(state, prev_keys, prev_values, prev_decay, prev_beta, accepted)
 
     vmem = pl.BlockSpec(memory_space=pltpu.VMEM)
     hbm = pl.BlockSpec(memory_space=pl.ANY)
@@ -395,10 +424,10 @@
     mixed = pl.pallas_call(
         functools.partial(verify_kernel, nkv, heads, steps),
         out_shape=jax.ShapeDtypeStruct((rows, feat), BF16),
-        in_specs=[vmem, vmem] + [hbm] * 6 + [vmem, vmem] + [hbm] * 2,
+        in_specs=[vmem] * (nkv + 1) + [hbm] * 6 + [vmem, vmem] + [hbm] * 2,
         out_specs=vmem,
         scratch_shapes=[
-            pltpu.VMEM((blocks, rows, feat), BF16),
+            pltpu.VMEM((nkv, rows, feat), BF16),
             pltpu.VMEM((4 * cols + 2 * allheads, full), BF16),
             pltpu.VMEM((cols, full), BF16),
             pltpu.VMEM((seqs, cols, width), F32),
@@ -416,7 +445,6 @@
             DMA((blocks, 6)),
             DMA((2,)),
             DMA((nkv,)),
-            DMA((blocks,)),
             DMA((nkv,)),
             DMA((2,)),
             DMA((2,)),
@@ -426,10 +454,11 @@
             DMA((nkv,)),
         ],
         compiler_params=pltpu.CompilerParams(
-            collective_id=0, has_side_effects=True, vmem_limit_bytes=60 * 1024 * 1024
+            collective_id=0, has_side_effects=True, vmem_limit_bytes=40 * 1024 * 1024
         ),
     )(
-        jnp.transpose(tokens, (1, 0, 2)).reshape(rows, feat),
+        flat,
+        *got,
         norm_gain.reshape(1, full),
         w_query.reshape(cols, full),
         w_key.reshape(cols, full),
@@ -437,8 +466,8 @@
         w_gate.reshape(cols, full),
         w_decay.T,
         w_beta.T,
-        jnp.repeat(decay_rate, group).reshape(1, cols),
-        jnp.tile(head_gain, heads).reshape(1, cols),
+        decay_rate.reshape(1, heads),
+        head_gain.reshape(1, group),
         w_out.reshape(cols, full),
         committed,
     )

time: 49.3 us -> 45.3 us (0.919)
  Pallas kernels: 38.7 us -> 27.3 us
  starting transfers between devices: 0 us -> 7.04 us
  local copies, waits for them, and re-layouts: 7.26 us -> 9.88 us
  other arithmetic: 2.3 us -> 0 us
    pallas_call x1, Pallas kernels: 33.2 us -> 21.3 us  [local(): pl.pallas_call(functools.partial(verify_kernel, nkv, heads, steps), out_s...]
    unnamed x6 -> x22, local copies, waits for them, and re-layouts: 0.01 us -> 8.27 us
    ppermute x0 -> x3, starting transfers between devices: none -> 7.04 us  [local(): lax.ppermute(flat, 'kv', [((i + d) % nkv, i) for i in range(nkv)])]
    reshape x5 -> x0, local copies, waits for them, and re-layouts: 3.01 us -> none  [the longest x2 1.6 us: wide(): jnp.broadcast_to(x, (steps, seqs, heads, group)).reshape(steps, seqs, cols)]
    another operation x3 -> x0, local copies, waits for them, and re-layouts: 1.32 us -> none  [the longest x2 0.66 us: local(): jnp.tile(head_gain, heads).reshape(1, cols)]
    reshape x1 -> x0, other arithmetic: 0.91 us -> none  [commit(): jnp.transpose(prev_values, (1, 0, 2, 3)).astype(F32)]
    reshape x1, local copies, waits for them, and re-layouts: 1.58 us -> 0.69 us  [local(): mixed = jnp.transpose(mixed.reshape(steps, seqs, feat), (1, 0, 2))]
    transpose x1 -> x0, other arithmetic: 0.73 us -> none  [wide(): x = jnp.transpose(x, (1, 0, 2))[..., None]]
  transfers between devices with their start and end apart: 0 -> 3, of which waited for: 0 -> 0; matrix products, arithmetic and copies ran while one was open for 0% -> 0% of each run, Pallas kernels for 0% -> 13%
where the time goes in v1:
time: 45.3 us; the launch traced here: 45 us
  Pallas kernels  27.3 us (60%)
  local copies, waits for them, and re-layouts  9.88 us (22%)
  starting transfers between devices  7.04 us (16%)
  between operations  0.73 us (2%)
    pallas_call x1, Pallas kernels, local(): pl.pallas_call(functools.partial(verify_kernel, nkv, heads, steps), out_s...  21.3 us
    unnamed x22, local copies, waits for them, and re-layouts  8.27 us
    ppermute x3, starting transfers between devices, local(): lax.ppermute(flat, 'kv', [((i + d) % nkv, i) for i in range(nkv)])  7.04 us
    pallas_call x1, Pallas kernels, commit(): pl.pallas_call(functools.partial(commit_kernel, steps, heads), grid=(seqs...  5.99 us
    transpose x1, local copies, waits for them, and re-layouts, local(): flat = jnp.transpose(tokens, (1, 0, 2)).reshape(rows, feat)  0.91 us
  transfers between devices with their start and end apart: 3, of which 0 were waited for; matrix products, arithmetic and copies ran while one was open for 0% of the time, Pallas kernels for 13%

profile of v1, /device:TPU:0, one launch (start us, length us, event | category | flops | bytes accessed | tf_op | source)
XLA Modules:
  0.0 45.0 jit_solution(7323167109341564700)
XLA Ops:
  0.6 0.9 %copy.19 = bf16[4,24,512]{2,1,0:T(8,128)(2,1)S(1)} copy(bf16[4,24,512]{2,0,1:T(4,128)(2,1)} %bitcast.44) | data formatting | bytes 196608 | tf_op jit(solution)/shard_map/transpose | solution.py:413
  1.5 3.1 %collective-permute-start.2 = (bf16[96,512]{1,0:T(8,128)(2,1)S(1)}, bf16[96,512]{1,0:T(8,128)(2,1)S(1)}, u32[]{:S(2)}, u32[]{:S(2)}) collective-permute-start(bf16[96,512]{1,0:T(8,128)(2,1)S(1)} %bitcast.33), channel_id=1, source_target_pairs={{6,0},{0,2},{2,4},{4,6},{7,1},{1,3},{3,5},{5,7},{14,8},{8,10},{10,... | collective-permute-start | bytes 294920 | tf_op jit(solution)/shard_map/ppermute | solution.py:415
  4.6 2.6 %collective-permute-start.1 = (bf16[96,512]{1,0:T(8,128)(2,1)S(1)}, bf16[96,512]{1,0:T(8,128)(2,1)S(1)}, u32[]{:S(2)}, u32[]{:S(2)}) collective-permute-start(bf16[96,512]{1,0:T(8,128)(2,1)S(1)} %bitcast.34), channel_id=1, source_target_pairs={{4,0},{6,2},{0,4},{2,6},{5,1},{7,3},{1,5},{3,7},{12,8},{14,10},{8,... | collective-permute-start | bytes 294920 | tf_op jit(solution)/shard_map/ppermute | solution.py:415
  7.2 1.3 %collective-permute-start = (bf16[96,512]{1,0:T(8,128)(2,1)S(1)}, bf16[96,512]{1,0:T(8,128)(2,1)S(1)}, u32[]{:S(2)}, u32[]{:S(2)}) collective-permute-start(bf16[96,512]{1,0:T(8,128)(2,1)S(1)} %bitcast.35), channel_id=1, source_target_pairs={{2,0},{4,2},{6,4},{0,6},{3,1},{5,3},{7,5},{1,7},{10,8},{12,10},{14... | collective-permute-start | bytes 294920 | tf_op jit(solution)/shard_map/ppermute | solution.py:415
  8.6 0.0 copy-start.1
  8.6 0.0 copy-start.6
  8.6 0.0 copy-start.7
  8.6 0.0 copy-start.8
  8.6 0.0 copy-start.9
  8.6 0.0 copy-start.10
  8.6 6.0 %shard_map.176.refs_13_ = f32[24,256,128]{2,1,0:T(8,128)} custom-call(bf16[384,128]{1,0:T(8,128)(2,1)} %bitcast.46, bf16[384,64]{1,0:T(8,128)(2,1)} %bitcast.47, f32[16,24]{1,0:T(8,128)} %bitcast.48, f32[16,24]{1,0:T(8,128)} %bitcast.49, s32[1,24]{1,0:T(1,128)} %bitcast.50, f32[24,256,128]{2,1,0:T(8,128)} %bitcast.43), custom_call_target="tpu_custom_call" | custom-call | flops 50331648 | bytes 6291456 | tf_op jit(solution)/shard_map/pallas_call | solution.py:147
  14.6 0.0 collective-permute-done.2.refs_2_
  14.6 0.0 collective-permute-done.1.refs_1_
  14.6 0.0 collective-permute-done.refs_0_
  14.6 0.0 copy-done.1
  14.6 0.0 copy-done.6
  14.7 0.0 copy-done.7
  14.7 0.0 copy-done.8
  14.7 0.0 copy-done.9
  14.7 0.0 copy-done.10
  14.7 0.0 copy-start
  14.7 1.9 %copy-done = f32[24,256,128]{2,1,0:T(8,128)S(1)} copy-done((f32[24,256,128]{2,1,0:T(8,128)S(1)}, f32[24,256,128]{2,1,0:T(8,128)}, u32[]{:S(2)}) %copy-start) | copy-done | bytes 3145752
  16.6 0.0 copy-start.2
  16.6 1.6 %copy-done.2 = bf16[4,64,4096]{2,1,0:T(8,128)(2,1)S(1)} copy-done((bf16[4,64,4096]{2,1,0:T(8,128)(2,1)S(1)}, bf16[4,64,4096]{2,1,0:T(8,128)(2,1)}, u32[]{:S(2)}) %copy-start.2) | copy-done | bytes 2097176
  18.2 0.0 copy-start.3
  18.2 1.6 %copy-done.3 = bf16[4,64,4096]{2,1,0:T(8,128)(2,1)S(1)} copy-done((bf16[4,64,4096]{2,1,0:T(8,128)(2,1)S(1)}, bf16[4,64,4096]{2,1,0:T(8,128)(2,1)}, u32[]{:S(2)}) %copy-start.3) | copy-done | bytes 2097176
  19.8 0.0 copy-start.4
  19.8 1.6 %copy-done.4 = bf16[4,64,4096]{2,1,0:T(8,128)(2,1)S(1)} copy-done((bf16[4,64,4096]{2,1,0:T(8,128)(2,1)S(1)}, bf16[4,64,4096]{2,1,0:T(8,128)(2,1)}, u32[]{:S(2)}) %copy-start.4) | copy-done | bytes 2097176
  21.4 0.0 copy-start.5
  21.4 1.6 %copy-done.5 = bf16[4,64,4096]{2,1,0:T(8,128)(2,1)S(1)} copy-done((bf16[4,64,4096]{2,1,0:T(8,128)(2,1)S(1)}, bf16[4,64,4096]{2,1,0:T(8,128)(2,1)}, u32[]{:S(2)}) %copy-start.5) | copy-done | bytes 2097176
  23.0 21.3 %shard_map.177 = bf16[96,512]{1,0:T(8,128)(2,1)S(1)} custom-call(bf16[96,512]{1,0:T(8,128)(2,1)S(1)} %bitcast.36, bf16[96,512]{1,0:T(8,128)(2,1)S(1)} %collective-permute-done.refs_0_, bf16[96,512]{1,0:T(8,128)(2,1)S(1)} %collective-permute-done.1.refs_1_, bf16[96,512]{1,0:T(8,128)(2,1)S(1)} %collective-permute-done.2.refs_2_, f32[1,4096]{1,0:T(1,128)S(1)} %bitcast.40, ...), custom_call_target="tpu_custom_call" | custom-call | tf_op jit(solution)/shard_map/pallas_call | solution.py:424
  44.3 0.7 %copy.22 = bf16[4,24,512]{2,0,1:T(4,128)(2,1)} copy(bf16[4,24,512]{2,1,0:T(8,128)(2,1)S(1)} %bitcast.37) | data formatting | bytes 196608 | tf_op jit(solution)/shard_map/reshape | solution.py:474
Async XLA Ops:
  1.5 13.1 %collective-permute-start.2 = (bf16[96,512]{1,0:T(8,128)(2,1)S(1)}, bf16[96,512]{1,0:T(8,128)(2,1)S(1)}, u32[]{:S(2)}, u32[]{:S(2)}) collective-permute-start(bf16[96,512]{1,0:T(8,128)(2,1)S(1)} %bitcast.33), channel_id=1, source_target_pairs={{6,0},{0,2},{2,4},{4,6},{7,1},{1,3},{3,5},{5,7},{14,8},{8,10},{10,... | collective-permute-start | bytes 294920 | tf_op jit(solution)/shard_map/ppermute | solution.py:415
  4.6 10.0 %collective-permute-start.1 = (bf16[96,512]{1,0:T(8,128)(2,1)S(1)}, bf16[96,512]{1,0:T(8,128)(2,1)S(1)}, u32[]{:S(2)}, u32[]{:S(2)}) collective-permute-start(bf16[96,512]{1,0:T(8,128)(2,1)S(1)} %bitcast.34), channel_id=1, source_target_pairs={{4,0},{6,2},{0,4},{2,6},{5,1},{7,3},{1,5},{3,7},{12,8},{14,10},{8,... | collective-permute-start | bytes 294920 | tf_op jit(solution)/shard_map/ppermute | solution.py:415
  7.2 7.4 %collective-permute-start = (bf16[96,512]{1,0:T(8,128)(2,1)S(1)}, bf16[96,512]{1,0:T(8,128)(2,1)S(1)}, u32[]{:S(2)}, u32[]{:S(2)}) collective-permute-start(bf16[96,512]{1,0:T(8,128)(2,1)S(1)} %bitcast.35), channel_id=1, source_target_pairs={{2,0},{4,2},{6,4},{0,6},{3,1},{5,3},{7,5},{1,7},{10,8},{12,10},{14... | collective-permute-start | bytes 294920 | tf_op jit(solution)/shard_map/ppermute | solution.py:415
  8.6 6.0 %copy-start.1 = (bf16[4,64,4096]{2,1,0:T(8,128)(2,1)S(1)}, bf16[4,64,4096]{2,1,0:T(8,128)(2,1)}, u32[]{:S(2)}) copy-start(bf16[4,64,4096]{2,1,0:T(8,128)(2,1)} %param.19) | copy-start | bytes 6291460
  8.6 6.1 %copy-start.6 = (bf16[4096,16]{0,1:T(8,128)(2,1)S(1)}, bf16[4096,16]{0,1:T(8,128)(2,1)}, u32[]{:S(2)}) copy-start(bf16[4096,16]{0,1:T(8,128)(2,1)} %param.23) | copy-start | bytes 393220
  8.6 6.1 %copy-start.7 = (bf16[4096,16]{0,1:T(8,128)(2,1)S(1)}, bf16[4096,16]{0,1:T(8,128)(2,1)}, u32[]{:S(2)}) copy-start(bf16[4096,16]{0,1:T(8,128)(2,1)} %param.24) | copy-start | bytes 393220
  8.6 6.1 %copy-start.8 = (f32[4096]{0:T(1024)S(1)}, f32[4096]{0:T(1024)}, u32[]{:S(2)}) copy-start(f32[4096]{0:T(1024)} %param.18) | copy-start | bytes 49156
  8.6 6.1 %copy-start.9 = (f32[4]{0:T(128)S(1)}, f32[4]{0:T(128)}, u32[]{:S(2)}) copy-start(f32[4]{0:T(128)} %param.25) | copy-start | bytes 52
  8.6 6.1 %copy-start.10 = (f32[64]{0:T(128)S(1)}, f32[64]{0:T(128)}, u32[]{:S(2)}) copy-start(f32[64]{0:T(128)} %param.26) | copy-start | bytes 772
  14.7 1.9 %copy-start = (f32[24,256,128]{2,1,0:T(8,128)S(1)}, f32[24,256,128]{2,1,0:T(8,128)}, u32[]{:S(2)}) copy-start(f32[24,256,128]{2,1,0:T(8,128)} %shard_map.176.refs_13_) | copy-start | bytes 9437188
  16.6 1.6 %copy-start.2 = (bf16[4,64,4096]{2,1,0:T(8,128)(2,1)S(1)}, bf16[4,64,4096]{2,1,0:T(8,128)(2,1)}, u32[]{:S(2)}) copy-start(bf16[4,64,4096]{2,1,0:T(8,128)(2,1)} %param.20) | copy-start | bytes 6291460
  18.2 1.6 %copy-start.3 = (bf16[4,64,4096]{2,1,0:T(8,128)(2,1)S(1)}, bf16[4,64,4096]{2,1,0:T(8,128)(2,1)}, u32[]{:S(2)}) copy-start(bf16[4,64,4096]{2,1,0:T(8,128)(2,1)} %param.21) | copy-start | bytes 6291460
  19.8 1.6 %copy-start.4 = (bf16[4,64,4096]{2,1,0:T(8,128)(2,1)S(1)}, bf16[4,64,4096]{2,1,0:T(8,128)(2,1)}, u32[]{:S(2)}) copy-start(bf16[4,64,4096]{2,1,0:T(8,128)(2,1)} %param.22) | copy-start | bytes 6291460
  21.4 1.6 %copy-start.5 = (bf16[4,64,4096]{2,1,0:T(8,128)(2,1)S(1)}, bf16[4,64,4096]{2,1,0:T(8,128)(2,1)}, u32[]{:S(2)}) copy-start(bf16[4,64,4096]{2,1,0:T(8,128)(2,1)} %param.27) | copy-start | bytes 6291460

commit v2 on v1

--- a/solution.py
+++ b/solution.py
@@ -56,26 +56,27 @@
     return total
 
 
-def commit_kernel(steps, heads, k_ref, v_ref, pd_ref, pb_ref, acc_ref, s_ref, out_ref, kbuf, vbuf, pbuf, ubuf, coef):
+def coefficients(steps, heads, cols, pd_ref, pb_ref, acc_ref, coef):
+    rows = steps * heads
+    group = cols // heads
+    total = acc_ref.shape[1]
+    step_of = lax.broadcasted_iota(jnp.int32, (rows, total), 0) // heads
+    mask = (step_of < acc_ref[...]).astype(F32)
+    retain = jnp.exp(-pd_ref[...] * mask)
+    beta = pb_ref[...] * mask
+    head_of = lax.broadcasted_iota(jnp.int32, (rows, cols), 0)
+    for t in range(steps):
+        pick = (head_of == t * heads + lane_group(rows, cols, group)).astype(F32)
+        for n, x in enumerate((retain, beta)):
+            coef[n * steps + t] = lax.dot_general(
+                x, pick, TN, precision=lax.Precision.HIGHEST, preferred_element_type=F32
+            )
+
+
+def commit_block(steps, heads, block, k_ref, v_ref, s_ref, out_ref, kbuf, vbuf, pbuf, ubuf, coef):
     seqs, cols, width = s_ref.shape
     group = cols // heads
     rows = steps * heads
-    total = acc_ref.shape[1]
-
-    @pl.when(pl.program_id(0) == 0)
-    def _():
-        step_of = lax.broadcasted_iota(jnp.int32, (rows, total), 0) // heads
-        mask = (step_of < acc_ref[...]).astype(F32)
-        retain = jnp.exp(-pd_ref[...] * mask)
-        beta = pb_ref[...] * mask
-        head_of = lax.broadcasted_iota(jnp.int32, (rows, cols), 0)
-        for t in range(steps):
-            pick = (head_of == t * heads + lane_group(rows, cols, group)).astype(F32)
-            for n, x in enumerate((retain, beta)):
-                coef[n * steps + t] = lax.dot_general(
-                    x, pick, TN, precision=lax.Precision.HIGHEST, preferred_element_type=F32
-                )
-
     kbuf[...] = k_ref[...].astype(F32)
     values = v_ref[...].astype(F32)
     vbuf[...] = jnp.concatenate([values] * (width // group), axis=1)
@@ -101,7 +102,7 @@
     )
     gram = {pair: sums[n * seqs : (n + 1) * seqs] for n, pair in enumerate(pairs)}
     norm = [lax.rsqrt(gram[(t, t)] + EPS) for t in range(steps)]
-    here = pl.ds(pl.multiple_of(pl.program_id(0) * seqs, seqs), seqs)
+    here = pl.ds(block * seqs, seqs)
     fed = []
     through = None
     copies = max(1, cols // width)
@@ -135,64 +136,17 @@
             out_ref[s, span, :] = kept * s_ref[s, span, :] + update[span]
 
 
-def commit(state, prev_keys, prev_values, prev_decay, prev_beta, accepted):
-    seqs, steps, heads, width = prev_keys.shape
-    group = state.shape[2]
-    cols = heads * group
-    block = 8
-    rows = steps * heads
-    big = pl.BlockSpec((block, cols, width), lambda i: (i, 0, 0))
-    coef = pl.BlockSpec((rows, seqs), lambda i: (0, 0))
-    tiles = pl.cdiv(cols, 128)
-    return pl.pallas_call(
-        functools.partial(commit_kernel, steps, heads),
-        grid=(seqs // block,),
-        out_shape=jax.ShapeDtypeStruct((seqs, cols, width), F32),
-        in_specs=[
-            pl.BlockSpec((block * rows, width), lambda i: (i, 0)),
-            pl.BlockSpec((block * rows, group), lambda i: (i, 0)),
-            coef,
-            coef,
-            pl.BlockSpec((1, seqs), lambda i: (0, 0)),
-            big,
-        ],
-        out_specs=big,
-        scratch_shapes=[
-            pltpu.VMEM((block * rows, width), F32),
-            pltpu.VMEM((block * rows, width), F32),
-            pltpu.VMEM((tiles, block * rows, 128), F32),
-            pltpu.VMEM((tiles, block * rows, 128), F32),
-            pltpu.VMEM((2 * steps, seqs, cols), F32),
-        ],
-        cost_estimate=pl.CostEstimate(
-            flops=4 * seqs * rows * cols * width, bytes_accessed=8 * state.size, transcendentals=0
-        ),
-    )(
-        prev_keys.reshape(seqs * rows, width),
-        prev_values.reshape(seqs * rows, group),
-        jnp.transpose(prev_decay, (1, 2, 0)).reshape(rows, seqs),
-        jnp.transpose(prev_beta, (1, 2, 0)).reshape(rows, seqs),
-        accepted.reshape(1, seqs),
-        state.reshape(seqs, cols, width),
-    )
-
-
 def verify_kernel(
-    nkv, heads, steps, tok_ref, *refs
-):
-    got, refs = refs[: nkv - 1], refs[nkv - 1 :]
-    verify(nkv, heads, steps, (tok_ref, *got), *refs)
-
-
-def verify(
     nkv, heads, steps,
-    got, gain_ref, wq_ref, wk_ref, wv_ref, wg_ref, wd_ref, wb_ref, rate_ref, hg_ref, wo_ref, st_ref,
-    out_ref,
+    tok_ref, gain_ref, wq_ref, wk_ref, wv_ref, wg_ref, wd_ref, wb_ref, rate_ref, hg_ref, wo_ref, st_ref,
+    ok_ref, ov_ref, pd_ref, pb_ref, acc_ref,
+    out_ref, com_ref,
     xs, w, wo, st, acc, halves, kbuf, pbuf, ssend, srecv, psend, precv, part, zsend, zrecv,
-    w_sem, big_sem, ag_send, ag_recv, ex_send, ex_recv, p_send, p_recv, z_send, z_recv,
+    ckbuf, cvbuf, cpbuf, cubuf, coef,
+    w_sem, big_sem, ag_send, ag_recv, fw_send, fw_recv, ex_send, ex_recv, p_send, p_recv, z_send, z_recv,
 ):
     kv, tp = lax.axis_index("kv"), lax.axis_index("tp")
-    rows, feat = got[0].shape
+    rows, feat = tok_ref.shape
     seqs, cols, width = st.shape
     group = cols // heads
     allheads = wd_ref.shape[0]
@@ -202,7 +156,9 @@
         return lax.rem(kv + d, nkv)
 
     hops = sorted(range(1, nkv), key=lambda d: (min(d, nkv - d), d))
-    order = [(d, e) for e in (0, 1) for d in [0] + hops]
+    early, late = hops[:2], hops[2:]
+    order = [(0, 0), (0, 1)] + [(d, 0) for d in early]
+    order += [(d, 1) for d in early] + [(d, e) for d in late for e in (0, 1)]
 
     def owner(d, e):
         return far(d) * 2 + (tp if e == 0 else 1 - tp)
@@ -228,12 +184,12 @@
     pl.semaphore_signal(barrier, inc=1, device_id=partner, device_id_type=MESH)
     for d in hops:
         pl.semaphore_signal(barrier, inc=1, device_id={"kv": far(d)}, device_id_type=MESH)
+    st_copy = pltpu.make_async_copy(st_ref, st, big_sem.at[0])
+    wo_copy = pltpu.make_async_copy(wo_ref, wo, big_sem.at[1])
+    st_copy.start()
     for chunk in loads:
         for copy in chunk:
             copy.start()
-    st_copy = pltpu.make_async_copy(st_ref, st, big_sem.at[0])
-    wo_copy = pltpu.make_async_copy(wo_ref, wo, big_sem.at[1])
-    st_copy.start()
     wo_copy.start()
     pl.semaphore_wait(barrier, nkv)
 
@@ -242,20 +198,43 @@
             src_ref=src, dst_ref=dst, send_sem=send, recv_sem=recv, device_id=where, device_id_type=MESH
         )
 
-    pending = []
-    for d in [0] + hops:
-        copy = remote(got[d], xs.at[d], ag_send.at[d], ag_recv.at[d], partner)
-        copy.start()
-        pending.append(copy)
+    direct, passed = {}, {}
+    for d in hops:
+        direct[d] = remote(tok_ref, xs.at[d, 0], ag_send.at[d], ag_recv.at[d], {"kv": lax.rem(kv + nkv - d, nkv)})
+        direct[d].start()
+    passed[0] = remote(tok_ref, xs.at[0, 1], fw_send.at[0], fw_recv.at[0], partner)
+    passed[0].start()
+
+    def hand_on(d):
+        direct[d].wait_recv()
+        passed[d] = remote(xs.at[d, 0], xs.at[d, 1], fw_send.at[d], fw_recv.at[d], partner)
+        passed[d].start()
+
+    coefficients(steps, heads, cols, pd_ref, pb_ref, acc_ref, coef)
+    st_copy.wait()
+    block = 8
+    for i in range(seqs // block):
+        few = pl.ds(i * block, block)
+        held = pl.ds(i * block * steps * heads, block * steps * heads)
+        commit_block(
+            steps, heads, i, ok_ref.at[held], ov_ref.at[held], st.at[few], com_ref.at[few],
+            ckbuf, cvbuf, cpbuf, cubuf, coef,
+        )
+    for d in early:
+        hand_on(d)
 
     square = jnp.zeros((rows, 1), F32)
     for n, (d, e) in enumerate(order):
         block = owner(d, e)
-        if e == 0:
-            x = got[d][...]
+        if n == 2 + len(early):
+            for far_d in late:
+                hand_on(far_d)
+        if n == 0:
+            x = tok_ref[...]
         else:
-            pending[[0, *hops].index(d)].wait_recv()
-            x = xs[d]
+            if e == 1:
+                passed[d].wait_recv()
+            x = xs[d, e]
         x = x.astype(F32)
         square = square + jnp.sum(x * x, axis=1, keepdims=True)
         xg = (x * gain_ref[:, span(block)]).astype(BF16)
@@ -312,11 +291,10 @@
             place = (h * 2) * steps + t
             kbuf[pl.ds(place, seqs, stride=heads * 2 * steps), :] = at(key, t)[:, lanes]
             kbuf[pl.ds(place + steps, seqs, stride=heads * 2 * steps), :] = at(query, t)[:, lanes]
-    st_copy.wait()
     tall = 2 * steps
     for s in range(seqs):
         stacked = kbuf[pl.ds(s * heads * tall, heads * tall), :].astype(BF16)
-        seen = dot_nt(stacked, st[s].astype(BF16))
+        seen = dot_nt(stacked, com_ref[s].astype(BF16))
         put(
             pbuf,
             pl.ds(s * tall, tall),
@@ -380,7 +358,7 @@
         copy.wait_recv()
         mixed = mixed + zrecv[j].astype(F32)
     out_ref[...] = mixed.astype(BF16)
-    for copy in pending + pending_tail + crossing + flights:
+    for copy in [*direct.values(), *passed.values()] + pending_tail + crossing + flights:
         copy.wait_send()
 
 
@@ -410,24 +388,23 @@
     rows = seqs * steps
     full = norm_gain.shape[0]
     allheads = w_decay.shape[1]
-    flat = jnp.transpose(tokens, (1, 0, 2)).reshape(rows, feat)
-    got = [
-        lax.ppermute(flat, "kv", [((i + d) % nkv, i) for i in range(nkv)]) for d in range(1, nkv)
-    ]
-    committed = commit(state, prev_keys, prev_values, prev_decay, prev_beta, accepted)
-
     vmem = pl.BlockSpec(memory_space=pltpu.VMEM)
-    hbm = pl.BlockSpec(memory_space=pl.ANY)
+    hbm = pl.BlockSpec(memory_space=pltpu.HBM)
+    tiles = pl.cdiv(cols, 128)
+    old = 8 * steps * heads
     blocks = 2 * nkv
     tall = 2 * steps
     DMA = pltpu.SemaphoreType.DMA
-    mixed = pl.pallas_call(
+    mixed, committed = pl.pallas_call(
         functools.partial(verify_kernel, nkv, heads, steps),
-        out_shape=jax.ShapeDtypeStruct((rows, feat), BF16),
-        in_specs=[vmem] * (nkv + 1) + [hbm] * 6 + [vmem, vmem] + [hbm] * 2,
-        out_specs=vmem,
+        out_shape=(
+            jax.ShapeDtypeStruct((rows, feat), BF16),
+            pltpu.VMEM((seqs, cols, width), F32),
+        ),
+        in_specs=[vmem] * 2 + [hbm] * 6 + [vmem, vmem] + [hbm] * 2 + [vmem] * 5,
+        out_specs=(vmem, vmem),
         scratch_shapes=[
-            pltpu.VMEM((nkv, rows, feat), BF16),
+            pltpu.VMEM((nkv, 2, rows, feat), BF16),
             pltpu.VMEM((4 * cols + 2 * allheads, full), BF16),
             pltpu.VMEM((cols, full), BF16),
             pltpu.VMEM((seqs, cols, width), F32),
@@ -442,10 +419,17 @@
             pltpu.VMEM((nkv, rows, feat), F32),
             pltpu.VMEM((nkv, rows, feat), BF16),
             pltpu.VMEM((nkv, rows, feat), BF16),
+            pltpu.VMEM((old, width), F32),
+            pltpu.VMEM((old, width), F32),
+            pltpu.VMEM((tiles, old, 128), F32),
+            pltpu.VMEM((tiles, old, 128), F32),
+            pltpu.VMEM((2 * steps, seqs, cols), F32),
             DMA((blocks, 6)),
             DMA((2,)),
             DMA((nkv,)),
             DMA((nkv,)),
+            DMA((nkv,)),
+            DMA((nkv,)),
             DMA((2,)),
             DMA((2,)),
             DMA((nkv,)),
@@ -454,11 +438,10 @@
             DMA((nkv,)),
         ],
         compiler_params=pltpu.CompilerParams(
-            collective_id=0, has_side_effects=True, vmem_limit_bytes=40 * 1024 * 1024
+            collective_id=0, has_side_effects=True, vmem_limit_bytes=57 * 1024 * 1024
         ),
     )(
-        flat,
-        *got,
+        jnp.transpose(tokens, (1, 0, 2)).reshape(rows, feat),
         norm_gain.reshape(1, full),
         w_query.reshape(cols, full),
         w_key.reshape(cols, full),
@@ -469,7 +452,12 @@
         decay_rate.reshape(1, heads),
         head_gain.reshape(1, group),
         w_out.reshape(cols, full),
-        committed,
+        state.reshape(seqs, cols, width),
+        prev_keys.reshape(seqs * steps * heads, width),
+        prev_values.reshape(seqs * steps * heads, group),
+        jnp.transpose(prev_decay, (1, 2, 0)).reshape(steps * heads, seqs),
+        jnp.transpose(prev_beta, (1, 2, 0)).reshape(steps * heads, seqs),
+        accepted.reshape(1, seqs),
     )
     mixed = jnp.transpose(mixed.reshape(steps, seqs, feat), (1, 0, 2))
     return mixed, committed.reshape(state.shape)

time: 45.3 us -> 39.5 us (0.87)
  starting transfers between devices: 7.04 us -> 0 us
  Pallas kernels: 27.3 us -> 33.8 us
  local copies, waits for them, and re-layouts: 9.88 us -> 4.8 us
    pallas_call x1, Pallas kernels: 21.3 us -> 33.8 us  [local(): pl.pallas_call(functools.partial(verify_kernel, nkv, heads, steps), out_s...]
    ppermute x3 -> x0, starting transfers between devices: 7.04 us -> none  [local(): lax.ppermute(flat, 'kv', [((i + d) % nkv, i) for i in range(nkv)])]
    unnamed x22 -> x1, local copies, waits for them, and re-layouts: 8.27 us -> 1.66 us
    pallas_call x1 -> x0, Pallas kernels: 5.99 us -> none  [commit(): pl.pallas_call(functools.partial(commit_kernel, steps, heads), grid=(seqs...]
    reshape x1, local copies, waits for them, and re-layouts: 0.69 us -> 1.58 us  [local(): mixed = jnp.transpose(mixed.reshape(steps, seqs, feat), (1, 0, 2))]
    transpose x1, local copies, waits for them, and re-layouts: 0.91 us -> 1.55 us  [local(): jnp.transpose(tokens, (1, 0, 2)).reshape(rows, feat)]
  transfers between devices with their start and end apart: 3 -> 0, of which waited for: 0 -> 0; matrix products, arithmetic and copies ran while one was open for 0% -> 0% of each run, Pallas kernels for 13% -> 0%
where the time goes in v2:
time: 39.5 us; the launch traced here: 39.3 us
  Pallas kernels  33.8 us (86%)
  local copies, waits for them, and re-layouts  4.8 us (12%)
  between operations  0.64 us (2%)
    pallas_call x1, Pallas kernels, local(): pl.pallas_call(functools.partial(verify_kernel, nkv, heads, steps), out_s...  33.8 us
    unnamed x1, local copies, waits for them, and re-layouts  1.66 us
    reshape x1, local copies, waits for them, and re-layouts, local(): mixed = jnp.transpose(mixed.reshape(steps, seqs, feat), (1, 0, 2))  1.58 us
    transpose x1, local copies, waits for them, and re-layouts, local(): jnp.transpose(tokens, (1, 0, 2)).reshape(rows, feat)  1.55 us

profile of v2, /device:TPU:0, one launch (start us, length us, event | category | flops | bytes accessed | tf_op | source)
XLA Modules:
  0.0 39.3 jit_solution(5269035715566158234)
XLA Ops:
  0.6 1.6 %copy.19 = bf16[4,24,512]{2,1,0:T(8,128)(2,1)} copy(bf16[4,24,512]{2,0,1:T(4,128)(2,1)} %bitcast.39) | data formatting | bytes 196608 | tf_op jit(solution)/shard_map/transpose | solution.py:444
  2.2 33.8 %shard_map.176 = (bf16[96,512]{1,0:T(8,128)(2,1)}, f32[24,256,128]{2,1,0:T(8,128)S(1)}) custom-call(bf16[96,512]{1,0:T(8,128)(2,1)} %bitcast.34, f32[1,4096]{1,0:T(1,128)} %bitcast.42, bf16[256,4096]{1,0:T(8,128)(2,1)} %bitcast.29, bf16[256,4096]{1,0:T(8,128)(2,1)} %bitcast.30, bf16[256,4096]{1,0:T(8,128)(2,1)} %bitcast.31, bf16[256,4096]{1,0:T(8,128)(2,1)} %bitcast.32, ...), custom_call_target="tpu_custom_call" | custom-call | tf_op jit(solution)/shard_map/pallas_call | solution.py:398
  36.0 1.6 %copy.22 = bf16[4,24,512]{2,0,1:T(4,128)(2,1)} copy(bf16[4,24,512]{2,1,0:T(8,128)(2,1)} %bitcast.41) | data formatting | bytes 196608 | tf_op jit(solution)/shard_map/reshape | solution.py:462
  37.6 1.7 %copy.24 = f32[24,4,64,128]{3,2,1,0:T(8,128)} copy(f32[24,4,64,128]{3,2,1,0:T(8,128)S(1)} %bitcast.27) | data formatting | bytes 6291456

commit v3 on v2

--- a/solution.py
+++ b/solution.py
@@ -337,22 +337,28 @@
     scaled = (ready * lax.rsqrt(total / (2 * group) + EPS)).astype(BF16)
 
     targets = sorted(range(1, nkv), key=lambda d: (-min(d, nkv - d), d)) + [0]
-    crossing = []
+    crossing, flights = [], []
+
+    def chip_sum(j):
+        crossing[j].wait_recv()
+        both = part[j] + precv[j].astype(F32)
+        if targets[j]:
+            zsend[j] = both.astype(BF16)
+            copy = remote(zsend.at[j], zrecv.at[j], z_send.at[j], z_recv.at[j], {"kv": far(targets[j])})
+            copy.start()
+            flights.append(copy)
+        return both
+
     for j, d in enumerate(targets):
         psend[j] = jnp.dot(scaled, wo[:, span(owner(d, 1))], preferred_element_type=F32).astype(BF16)
         copy = remote(psend.at[j], precv.at[j], p_send.at[j], p_recv.at[j], partner)
         copy.start()
         crossing.append(copy)
         part[j] = jnp.dot(scaled, wo[:, span(owner(d, 0))], preferred_element_type=F32)
-    flights = []
-    for j, d in enumerate(targets):
-        crossing[j].wait_recv()
-        both = part[j] + precv[j].astype(F32)
-        if d:
-            zsend[j] = both.astype(BF16)
-            copy = remote(zsend.at[j], zrecv.at[j], z_send.at[j], z_recv.at[j], {"kv": far(d)})
-            copy.start()
-            flights.append(copy)
+        if j >= 2:
+            chip_sum(j - 2)
+    for j in range(max(0, nkv - 2), nkv):
+        both = chip_sum(j)
     mixed = both
     for j, copy in sorted(enumerate(flights), key=lambda f: -f[0]):
         copy.wait_recv()
@@ -398,7 +404,7 @@
     mixed, committed = pl.pallas_call(
         functools.partial(verify_kernel, nkv, heads, steps),
         out_shape=(
-            jax.ShapeDtypeStruct((rows, feat), BF16),
+            pltpu.VMEM((rows, feat), BF16),
             pltpu.VMEM((seqs, cols, width), F32),
         ),
         in_specs=[vmem] * 2 + [hbm] * 6 + [vmem, vmem] + [hbm] * 2 + [vmem] * 5,
@@ -441,7 +447,9 @@
             collective_id=0, has_side_effects=True, vmem_limit_bytes=57 * 1024 * 1024
         ),
     )(
-        jnp.transpose(tokens, (1, 0, 2)).reshape(rows, feat),
+        pltpu.with_memory_space_constraint(
+            jnp.transpose(tokens, (1, 0, 2)).reshape(rows, feat), pltpu.VMEM
+        ),
         norm_gain.reshape(1, full),
         w_query.reshape(cols, full),
         w_key.reshape(cols, full),

time: 39.5 us -> 37.2 us (0.942)
  local copies, waits for them, and re-layouts: 4.8 us -> 3.27 us
  Pallas kernels: 33.8 us -> 33.1 us
    reshape x1, local copies, waits for them, and re-layouts: 1.58 us -> 0.69 us  [local(): mixed = jnp.transpose(mixed.reshape(steps, seqs, feat), (1, 0, 2))]
    pallas_call x1, Pallas kernels: 33.8 us -> 33.1 us  [local(): pl.pallas_call(functools.partial(verify_kernel, nkv, heads, steps), out_s...]
    transpose x1, local copies, waits for them, and re-layouts: 1.55 us -> 0.91 us  [local(): jnp.transpose(tokens, (1, 0, 2)).reshape(rows, feat)]
where the time goes in v3:
time: 37.2 us; the launch traced here: 37.1 us
  Pallas kernels  33.1 us (89%)
  local copies, waits for them, and re-layouts  3.27 us (9%)
  between operations  0.64 us (2%)
    pallas_call x1, Pallas kernels, local(): pl.pallas_call(functools.partial(verify_kernel, nkv, heads, steps), out_s...  33.1 us
    unnamed x1, local copies, waits for them, and re-layouts  1.66 us
    transpose x1, local copies, waits for them, and re-layouts, local(): jnp.transpose(tokens, (1, 0, 2)).reshape(rows, feat)  0.91 us

profile of v3, /device:TPU:0, one launch (start us, length us, event | category | flops | bytes accessed | tf_op | source)
XLA Modules:
  0.0 37.1 jit_solution(3684921746296806191)
XLA Ops:
  0.6 0.9 %copy.19 = bf16[4,24,512]{2,1,0:T(8,128)(2,1)S(1)} copy(bf16[4,24,512]{2,0,1:T(4,128)(2,1)} %bitcast.40) | data formatting | bytes 196608 | tf_op jit(solution)/shard_map/transpose | solution.py:451
  1.5 33.1 %shard_map.176 = (bf16[96,512]{1,0:T(8,128)(2,1)S(1)}, f32[24,256,128]{2,1,0:T(8,128)S(1)}) custom-call(bf16[96,512]{1,0:T(8,128)(2,1)S(1)} %bitcast.28, f32[1,4096]{1,0:T(1,128)} %bitcast.42, bf16[256,4096]{1,0:T(8,128)(2,1)} %bitcast.31, bf16[256,4096]{1,0:T(8,128)(2,1)} %bitcast.32, bf16[256,4096]{1,0:T(8,128)(2,1)} %bitcast.33, ...), custom_call_target="tpu_custom_call" | custom-call | tf_op jit(solution)/shard_map/pallas_call | solution.py:404
  34.7 0.7 %copy.22 = bf16[4,24,512]{2,0,1:T(4,128)(2,1)} copy(bf16[4,24,512]{2,1,0:T(8,128)(2,1)S(1)} %bitcast.29) | data formatting | bytes 196608 | tf_op jit(solution)/shard_map/reshape | solution.py:470
  35.4 1.7 %copy.24 = f32[24,4,64,128]{3,2,1,0:T(8,128)} copy(f32[24,4,64,128]{3,2,1,0:T(8,128)S(1)} %bitcast.27) | data formatting | bytes 6291456
